TPU v7x, 32 devices: a whole 2x2x4 slice. The times are simulated.
32 devices in a mesh: ep: 8 (over z, core), tp: 4 (over y, x).
Axes of the slice: x: 2, y: 2, z: 4, core: 2. Of those that a mesh axis runs over, the one named last changes fastest.
Arguments:
- tokens: bfloat16 [128, 2048], P('ep'), may hold values from -6 to 6
- attn_gain: float32 [2048], replicated, may hold values from 0.1 to 1.9
- query_weight: bfloat16 [2048, 2048], P('ep', 'tp'), may hold values from -0.125 to 0.125
- key_weight: bfloat16 [2048, 2048], P('ep', 'tp'), may hold values from -0.125 to 0.125
- value_weight: bfloat16 [2048, 2048], P('ep', 'tp'), may hold values from -0.125 to 0.125
- forget_weight: bfloat16 [2048, 16], P(None, 'tp'), may hold values from -0.125 to 0.125
- forget_bias: float32 [16], P('tp'), may hold values from -1 to 2
- cache_keys: bfloat16 [128, 16, 384, 128], P('ep', 'tp'), may hold values from -240 to 240
- cache_values: bfloat16 [128, 16, 384, 128], P('ep', 'tp'), may hold values from -6 to 6
- cache_gates: float32 [128, 16, 384], P('ep', 'tp'), may hold values from -768 to 0, as said below
- lengths: int32 [128], P('ep'), may hold values from 1 to 384
- output_weight: bfloat16 [2048, 2048], P('tp', 'ep'), may hold values from -0.125 to 0.125
- ffn_gain: float32 [2048], replicated, may hold values from 0.1 to 1.9
- dense_gate_proj: bfloat16 [2048, 2048], P('ep', 'tp'), may hold values from -0.125 to 0.125
- dense_up_proj: bfloat16 [2048, 2048], P('ep', 'tp'), may hold values from -0.125 to 0.125
- dense_down_proj: bfloat16 [2048, 2048], P('tp', 'ep'), may hold values from -0.125 to 0.125
- dense_mix: bfloat16 [2048], replicated, may hold values from -0.125 to 0.125
- expert_ids: int32 [128, 2], P('ep'), may hold values from 0 to 7, as said below
- group_prob: float32 [128], P('ep'), may hold values from 0.25 to 1
- pair_prob: float32 [128, 2], P('ep'), may hold values from 0.05 to 1
- expert_gate: bfloat16 [8, 2048, 2048], P('ep', None, 'tp'), may hold values from -0.125 to 0.125
- expert_up: bfloat16 [8, 2048, 2048], P('ep', None, 'tp'), may hold values from -0.125 to 0.125
- expert_down: bfloat16 [8, 2048, 2048], P('ep', 'tp'), may hold values from -0.125 to 0.125
Outputs:
- mixed_out: bfloat16 [128, 2048], P('ep')
Inputs may be any that keep to these rules, and one draw needn't show every extreme that they name: `expert_ids`: each row names two different experts of one group, the groups being 4 runs of consecutive ids. In each aligned block of 16 rows (the rows of one index of ep) no expert is named more than 8 times, and some expert exactly 8 times. `cache_gates`: along positions the values never rise.
All inputs are finite; a program needn't handle non-finite values.
Results may differ from a plain program's by a relative error of at most 0.014.
Values may be sent and summed in bfloat16 or wider, within the bound.
A program may use at most 64 MiB of HBM per device.

v0:
```python
import math
import jax
import jax.numpy as jnp
from jax import lax
from jax.sharding import PartitionSpec as P

EPSILON = 1e-06


def rms_scale(values, norm_gain):
    widened = values.astype(jnp.float32)
    return (
        widened
        * lax.rsqrt(jnp.mean(widened * widened, axis=-1, keepdims=True) + EPSILON)
        * norm_gain
    )


def attend(queries, keys_new, values_new, key_cache, value_cache, gate_cache, lengths, log_forget):
    cache_span = key_cache.shape[2]
    score_scale = 1.0 / math.sqrt(key_cache.shape[3])
    positions = jnp.arange(cache_span, dtype=jnp.int32)
    live_mask = positions[None, :] < lengths[:, None]
    last_mask = positions[None, :] == lengths[:, None] - 1
    last_gate = jnp.sum(jnp.where(last_mask[:, None, :], gate_cache, 0.0), axis=-1)
    gate_now = last_gate + log_forget
    scores = (
        jnp.einsum("shd,shpd->shp", queries, key_cache, preferred_element_type=jnp.float32)
        * score_scale
    )
    scores = scores + gate_now[:, :, None] - gate_cache
    scores = jnp.where(live_mask[:, None, :], scores, -jnp.inf)
    own_score = (
        jnp.sum(queries.astype(jnp.float32) * keys_new.astype(jnp.float32), axis=-1) * score_scale
    )
    row_top = jnp.maximum(jnp.max(scores, axis=-1), own_score)
    raised = jnp.exp(scores - row_top[:, :, None])
    own_raised = jnp.exp(own_score - row_top)
    totals = jnp.sum(raised, axis=-1) + own_raised
    weights_low = (raised / totals[:, :, None]).astype(jnp.bfloat16)
    own_prob = (own_raised / totals).astype(jnp.bfloat16)
    attended = jnp.einsum(
        "shp,shpd->shd", weights_low, value_cache, preferred_element_type=jnp.float32
    )
    attended = attended + own_prob.astype(jnp.float32)[:, :, None] * values_new.astype(jnp.float32)
    return attended.astype(jnp.bfloat16)


def row_term(spread, joined):
    return jnp.dot(spread, joined, preferred_element_type=jnp.float32)


def right_product(left_rows, weight_piece):
    return jnp.dot(left_rows, weight_piece, preferred_element_type=jnp.float32)


def shards(
    tokens,
    attn_gain,
    query_weight,
    key_weight,
    value_weight,
    forget_weight,
    forget_bias,
    cache_keys,
    cache_values,
    cache_gates,
    lengths,
    output_weight,
    ffn_gain,
    dense_gate_proj,
    dense_up_proj,
    dense_down_proj,
    dense_mix,
    expert_ids,
    group_prob,
    pair_prob,
    expert_gate,
    expert_up,
    expert_down,
):
    seq_count = tokens.shape[0]
    head_count = cache_keys.shape[1]
    head_size = cache_keys.shape[3]
    proj_width = query_weight.shape[1]
    normed = rms_scale(tokens, attn_gain).astype(jnp.bfloat16)
    spread = lax.all_to_all(normed, "ep", split_axis=1, concat_axis=0, tiled=True)
    joined = jnp.concatenate([query_weight, key_weight, value_weight], axis=1)
    summed = lax.psum_scatter(row_term(spread, joined), "ep", scatter_dimension=0, tiled=True)
    projected = (
        summed[:, :proj_width],
        summed[:, proj_width : 2 * proj_width],
        summed[:, 2 * proj_width :],
    )
    queries = projected[0].astype(jnp.bfloat16).reshape(seq_count, head_count, head_size)
    keys_new = projected[1].astype(jnp.bfloat16).reshape(seq_count, head_count, head_size)
    values_new = projected[2].astype(jnp.bfloat16).reshape(seq_count, head_count, head_size)
    log_forget = jax.nn.log_sigmoid(
        jnp.dot(normed, forget_weight, preferred_element_type=jnp.float32) + forget_bias
    )
    attended = attend(
        queries, keys_new, values_new, cache_keys, cache_values, cache_gates, lengths, log_forget
    )
    attended = attended.reshape(seq_count, head_count * head_size)
    head_terms = right_product(attended, lax.all_gather(output_weight, "ep", axis=1, tiled=True))
    mixed_heads = lax.psum(head_terms, "tp")
    residual = (tokens.astype(jnp.float32) + mixed_heads).astype(jnp.bfloat16)
    ffn_in = rms_scale(residual, ffn_gain).astype(jnp.bfloat16)
    dense_width = dense_gate_proj.shape[1]
    ffn_spread = lax.all_to_all(ffn_in, "ep", split_axis=1, concat_axis=0, tiled=True)
    dense_joined = jnp.concatenate([dense_gate_proj, dense_up_proj], axis=1)
    dense_summed = lax.psum_scatter(
        row_term(ffn_spread, dense_joined).astype(jnp.bfloat16),
        "ep",
        scatter_dimension=0,
        tiled=True,
    ).astype(jnp.float32)
    dense_parts = (dense_summed[:, :dense_width], dense_summed[:, dense_width:])
    dense_hidden = (jax.nn.silu(dense_parts[0]) * dense_parts[1]).astype(jnp.bfloat16)
    dense_terms = right_product(
        dense_hidden, lax.all_gather(dense_down_proj, "ep", axis=1, tiled=True)
    )
    dense_total = lax.psum(dense_terms.astype(jnp.bfloat16), "tp").astype(jnp.float32)
    mix = jax.nn.sigmoid(jnp.dot(ffn_in, dense_mix, preferred_element_type=jnp.float32))
    expert_count = lax.axis_size("ep") * expert_gate.shape[0]
    capacity = 4 * seq_count // expert_count
    slot_total = expert_count * capacity
    picks = expert_ids.reshape(-1)
    expert_grid = jnp.arange(expert_count, dtype=jnp.int32)
    pick_onehot = (picks[:, None] == expert_grid[None, :]).astype(jnp.int32)
    earlier = jnp.cumsum(pick_onehot, axis=0) - pick_onehot
    slot_rank = jnp.sum(earlier * pick_onehot, axis=1)
    destination = (picks * capacity + slot_rank).reshape(seq_count, 2)
    slot_grid = jnp.arange(slot_total, dtype=jnp.int32)
    select_first = (destination[:, 0:1] == slot_grid[None, :]).astype(jnp.bfloat16)
    select_second = (destination[:, 1:2] == slot_grid[None, :]).astype(jnp.bfloat16)
    selector = select_first + select_second
    outbound = jnp.einsum("sk,sd->kd", selector, ffn_in, preferred_element_type=jnp.float32)
    outbound = outbound.astype(jnp.bfloat16).reshape(expert_count, capacity, ffn_in.shape[1])
    arrived = lax.all_to_all(outbound, "ep", split_axis=0, concat_axis=0, tiled=True)
    sources, slots_now, feature = arrived.shape
    row_data = arrived.reshape(sources * slots_now, feature)
    gate_part = jnp.dot(row_data, expert_gate[0], preferred_element_type=jnp.float32)
    up_part = jnp.dot(row_data, expert_up[0], preferred_element_type=jnp.float32)
    expert_hidden = (jax.nn.silu(gate_part) * up_part).astype(jnp.bfloat16)
    partial_out = jnp.dot(expert_hidden, expert_down[0], preferred_element_type=jnp.float32)
    expert_result = lax.psum(partial_out.astype(jnp.bfloat16), "tp").astype(jnp.float32)
    returned = lax.all_to_all(
        expert_result.reshape(sources, slots_now, feature).astype(jnp.bfloat16),
        "ep",
        split_axis=0,
        concat_axis=0,
        tiled=True,
    ).astype(jnp.float32)
    returned = returned.reshape(slot_total, ffn_in.shape[1])
    routes = group_prob[:, None] * pair_prob / jnp.sum(pair_prob, axis=1, keepdims=True)
    first_back = returned[destination[:, 0]]
    second_back = returned[destination[:, 1]]
    side_total = (
        routes[:, 0:1] * first_back + routes[:, 1:2] * second_back + mix[:, None] * dense_total
    )
    result = residual.astype(jnp.float32) + side_total
    return result.astype(jnp.bfloat16)


def solution(mesh):
    return jax.shard_map(
        shards,
        mesh=mesh,
        in_specs=(
            P("ep", None),
            P(),
            P("ep", "tp"),
            P("ep", "tp"),
            P("ep", "tp"),
            P(None, "tp"),
            P("tp"),
            P("ep", "tp", None, None),
            P("ep", "tp", None, None),
            P("ep", "tp", None),
            P("ep"),
            P("tp", "ep"),
            P(),
            P("ep", "tp"),
            P("ep", "tp"),
            P("tp", "ep"),
            P(),
            P("ep", None),
            P("ep"),
            P("ep", None),
            P("ep", None, "tp"),
            P("ep", None, "tp"),
            P("ep", "tp", None),
        ),
        out_specs=P("ep", None),
        check_vma=False,
    )
```

profile of v0, /device:TPU:0, one launch (start us, length us, event | category | flops | bytes accessed | tf_op | source)
XLA Modules:
  0.0 268.5 jit_solution(17298867801017753038)
XLA Ops:
  6.5 0.0 reduce-scatter.3.cloned.1.call-start
  6.6 1.1 fusion.32
  7.7 0.9 fusion.34
  8.7 12.1 %all_to_all.48 = bf16[16,8,256]{2,0,1:T(8,128)(2,1)S(1)} all-to-all(bf16[16,8,256]{2,0,1:T(8,128)(2,1)S(1)} %bitcast.96), channel_id=1, replica_groups=mesh['ep'=8,'tp'=4] {'ep'}, dimensions={1} | all-to-all | bytes 131072 | tf_op jit(solution)/shard_map/all_to_all | solution.py:87
  20.7 2.3 fusion.20
  23.0 0.0 reduce-scatter.3.cloned.1.call-update
  23.0 0.0 all-gather.3.cloned.1.call-start
  23.1 0.7 all-gather.3.cloned.1.call-update
  23.8 0.0 all-reduce.4.cloned.1.call-start
  23.8 0.0 copy-done.10
  23.9 0.1 iota_compare_fusion
  23.9 0.1 select_reduce_fusion
  24.0 0.1 copy.42
  24.1 0.0 copy-done.14
  24.1 0.1 fusion.70
  24.3 0.1 copy.43
  24.4 0.1 iota_compare_fusion.1
  24.4 29.2 %reduce-scatter.3.cloned.1.call-done = f32[16,1536]{1,0:T(8,128)} async-done(((f32[128,1536]{1,0:T(8,128)}), f32[16,1536]{1,0:T(8,128)}) %reduce-scatter.3.cloned.1.call-update) | async-done | bytes 98320 | tf_op jit(solution)/shard_map/reduce_scatter | solution.py:89
  53.6 0.9 convert.8
  54.6 0.1 multiply_reduce_fusion
  54.7 0.0 copy-start.1
  54.7 5.2 %fusion.80 = f32[16,4,1,384]{3,2,1,0:T(1,128)S(1)} fusion(bf16[16,4,128,1]{2,3,1,0:T(2,128)(2,1)S(1)} %reshape.151, bf16[16,4,384,128]{3,2,1,0:T(8,128)(2,1)} %param.30), kind=kOutput, calls=%fused_computation.117 | convolution fusion | flops 6291456 | bytes 6406144 | tf_op jit(solution)/shard_map/shd,shpd->shp/dot_general | solution.py:28
  59.9 0.2 fusion.78
  60.1 0.2 fusion.50
  60.3 0.1 fusion.52
  60.5 1.2 fusion.48
  61.7 0.0 copy-start.12
  61.7 0.1 add_convert_fusion
  61.8 22.4 %all-gather.3.cloned.1.call-done = bf16[512,2048]{1,0:T(8,128)(2,1)} async-done(((bf16[512,256]{1,0:T(8,128)(2,1)}), bf16[512,2048]{1,0:T(8,128)(2,1)}) %all-gather.3.cloned.1.call-update) | async-done | bytes 2097168 | tf_op jit(solution)/shard_map/all_gather | solution.py:105
  84.2 2.6 fusion.55
  86.8 0.0 all-reduce.4.cloned.1.call-update
  86.9 0.0 reduce-scatter.5.cloned.1.call-start
  86.9 41.4 %all-reduce.4.cloned.1.call-done = f32[16,2048]{1,0:T(8,128)} async-done(((f32[16,2048]{1,0:T(8,128)}), f32[16,2048]{1,0:T(8,128)}) %all-reduce.4.cloned.1.call-update) | async-done | bytes 131088 | tf_op jit(solution)/shard_map/psum | solution.py:106
  128.3 1.0 fusion.36
  129.4 0.1 fusion.38
  129.5 10.3 %all_to_all.49 = bf16[16,8,256]{2,0,1:T(8,128)(2,1)S(1)} all-to-all(bf16[16,8,256]{2,0,1:T(8,128)(2,1)S(1)} %bitcast.97), channel_id=1, replica_groups=mesh['ep'=8,'tp'=4] {'ep'}, dimensions={1} | all-to-all | bytes 131072 | tf_op jit(solution)/shard_map/all_to_all | solution.py:110
  139.8 0.9 convolution_convert_fusion.3
  140.8 0.0 reduce-scatter.5.cloned.1.call-update
  140.8 0.0 all-gather.5.cloned.1.call-start
  140.8 0.5 all-gather.5.cloned.1.call-update
  141.4 0.0 all-reduce.6.cloned.1.call-start
  141.4 0.1 copy.44
  141.5 0.1 eq.62
  141.6 0.1 fusion.59
  141.7 0.1 reduce_window_sum.11
  141.7 0.2 select_reduce_fusion.1
  141.9 0.1 reduce_sum.71
  142.0 0.1 copy.45
  142.1 0.3 fusion
  142.4 12.7 %all_to_all.50 = bf16[8,8,2048]{2,1,0:T(8,128)(2,1)S(1)} all-to-all(bf16[8,8,2048]{2,1,0:T(8,128)(2,1)S(1)} %fusion), channel_id=1, replica_groups=mesh['ep'=8,'tp'=4] {'ep'}, dimensions={0} | all-to-all | bytes 524288 | tf_op jit(solution)/shard_map/all_to_all | solution.py:140
  155.1 2.1 fusion.5
  157.2 3.2 %fusion.1 = bf16[8,8,2048]{2,1,0:T(8,128)(2,1)} fusion(bf16[1,512,2048]{2,1,0:T(8,128)(2,1)S(1)} %copy-done, bf16[1,2048,512]{2,1,0:T(8,128)(2,1)} %param.44, bf16[8,8,2048]{2,1,0:T(8,128)(2,1)S(1)} %all_to_all.50, f32[64,512]{1,0:T(8,128)S(1)} %fusion.5), kind=kOutput, calls=%fused_computation.5 | convolution fusion | flops 268763136 | bytes 4849664 | tf_op jit(solution)/shard_map/dot_general | solution.py:146
  160.5 9.1 %reduce-scatter.5.cloned.1.call-done = bf16[16,1024]{1,0:T(8,128)(2,1)} async-done(((bf16[128,1024]{1,0:T(8,128)(2,1)}), bf16[16,1024]{1,0:T(8,128)(2,1)}) %reduce-scatter.5.cloned.1.call-update) | async-done | bytes 32784 | tf_op jit(solution)/shard_map/reduce_scatter | solution.py:112
  169.6 0.8 convert_element_type.119
  170.3 29.4 %all-gather.5.cloned.1.call-done = bf16[512,2048]{1,0:T(8,128)(2,1)} async-done(((bf16[512,256]{1,0:T(8,128)(2,1)}), bf16[512,2048]{1,0:T(8,128)(2,1)}) %all-gather.5.cloned.1.call-update) | async-done | bytes 2097168 | tf_op jit(solution)/shard_map/all_gather | solution.py:121
  199.7 2.6 convolution_convert_fusion.2
  202.3 0.0 all-reduce.6.cloned.1.call-update
  202.4 42.8 %all-reduce.6.cloned.1.call-done = (bf16[16,2048]{1,0:T(8,128)(2,1)}, bf16[8,8,2048]{2,1,0:T(8,128)(2,1)}) async-done(((bf16[16,2048]{1,0:T(8,128)(2,1)}, bf16[8,8,2048]{2,1,0:T(8,128)(2,1)}), (bf16[16,2048]{1,0:T(8,128)(2,1)}, bf16[8,8,2048]{2,1,0:T(8,128)(2,1)})) %all-reduce.6.cloned.1.call-update) | async-done | bytes 327696 | tf_op jit(solution)/shard_map/psum | solution.py:123
  245.2 4.7 %all-to-all-start.2 = ((bf16[8,8,2048]{2,1,0:T(8,128)(2,1)}), bf16[8,8,2048]{2,1,0:T(8,128)(2,1)S(1)}, u32[]{:S(2)}, u32[]{:S(2)}) async-start(bf16[8,8,2048]{2,1,0:T(8,128)(2,1)} %get-tuple-element.6), calls=%async_computation.3 | async-start | bytes 524288 | tf_op jit(solution)/shard_map/all_to_all | solution.py:148
  250.0 0.1 fusion.17
  250.1 9.5 %all-to-all-done.2 = bf16[8,8,2048]{2,1,0:T(8,128)(2,1)S(1)} async-done(((bf16[8,8,2048]{2,1,0:T(8,128)(2,1)}), bf16[8,8,2048]{2,1,0:T(8,128)(2,1)S(1)}, u32[]{:S(2)}, u32[]{:S(2)}) %all-to-all-start.2) | async-done | bytes 262176 | tf_op jit(solution)/shard_map/all_to_all | solution.py:148
  259.7 0.6 gather_fusion
  260.3 0.6 gather_fusion.1
  260.9 0.7 fusion.39
  (46 shorter events, 0.3 us)
Async XLA Ops:
  6.5 150.7 %copy-start = (bf16[1,512,2048]{2,1,0:T(8,128)(2,1)S(1)}, bf16[1,512,2048]{2,1,0:T(8,128)(2,1)}, u32[]{:S(2)}) copy-start(bf16[1,512,2048]{2,1,0:T(8,128)(2,1)} %param.45) | copy-start | bytes 6291460
  6.5 17.3 %copy-start.10 = (s32[16]{0:T(128)S(1)}, s32[16]{0:T(128)}, u32[]{:S(2)}) copy-start(s32[16]{0:T(128)} %param.33) | copy-start | bytes 196
  6.5 17.4 %copy-start.3 = (f32[16,4,384]{2,1,0:T(4,128)S(1)}, f32[16,4,384]{2,1,0:T(4,128)}, u32[]{:S(2)}) copy-start(f32[16,4,384]{2,1,0:T(4,128)} %param.32) | copy-start | bytes 294916
  6.5 17.6 %copy-start.13 = (bf16[2048,4]{0,1:T(4,128)(2,1)S(1)}, bf16[2048,4]{0,1:T(4,128)(2,1)}, u32[]{:S(2)}) copy-start(bf16[2048,4]{0,1:T(4,128)(2,1)} %param.28) | copy-start | bytes 49156
  6.5 17.6 %copy-start.14 = (f32[4]{0:T(128)S(1)}, f32[4]{0:T(128)}, u32[]{:S(2)}) copy-start(f32[4]{0:T(128)} %param.29) | copy-start | bytes 52
  6.5 47.1 %reduce-scatter.3.cloned.1.call-start = ((), (), s32[]{:S(2)}) async-start(), calls=%async_computation.6 | async-start | bytes 884736 | tf_op jit(solution)/shard_map/reduce_scatter | solution.py:89
  23.0 61.2 %all-gather.3.cloned.1.call-start = ((), (), s32[]{:S(2)}) async-start(), calls=%async_computation.7 | async-start | bytes 2359296 | tf_op jit(solution)/shard_map/all_gather | solution.py:105
  23.8 104.6 %all-reduce.4.cloned.1.call-start = ((), (), s32[]{:S(2)}) async-start(), calls=%async_computation.8 | async-start | bytes 262144 | tf_op jit(solution)/shard_map/psum | solution.py:106
  54.7 5.8 %copy-start.1 = (bf16[16,4,384,128]{3,2,1,0:T(8,128)(2,1)S(1)}, bf16[16,4,384,128]{3,2,1,0:T(8,128)(2,1)}, u32[]{:S(2)}) copy-start(bf16[16,4,384,128]{3,2,1,0:T(8,128)(2,1)} %param.31) | copy-start | bytes 18874372
  61.7 66.7 %copy-start.2 = (bf16[16,2048]{1,0:T(8,128)(2,1)S(1)}, bf16[16,2048]{1,0:T(8,128)(2,1)}, u32[]{:S(2)}) copy-start(bf16[16,2048]{1,0:T(8,128)(2,1)} %param.23) | copy-start | bytes 196612
  61.7 67.7 %copy-start.5 = (f32[2048]{0:T(1024)S(1)}, f32[2048]{0:T(1024)}, u32[]{:S(2)}) copy-start(f32[2048]{0:T(1024)} %param.35) | copy-start | bytes 24580
  61.7 78.2 %copy-start.11 = (bf16[256,512]{1,0:T(8,128)(2,1)S(1)}, bf16[256,512]{1,0:T(8,128)(2,1)}, u32[]{:S(2)}) copy-start(bf16[256,512]{1,0:T(8,128)(2,1)} %param.37) | copy-start | bytes 786436
  61.7 78.1 %copy-start.12 = (bf16[256,512]{1,0:T(8,128)(2,1)S(1)}, bf16[256,512]{1,0:T(8,128)(2,1)}, u32[]{:S(2)}) copy-start(bf16[256,512]{1,0:T(8,128)(2,1)} %param.36) | copy-start | bytes 786436
  84.2 57.2 %copy-start.7 = (s32[16,2]{0,1:T(2,128)S(1)}, s32[16,2]{0,1:T(2,128)}, u32[]{:S(2)}) copy-start(s32[16,2]{0,1:T(2,128)} %param.40) | copy-start | bytes 388
  86.9 82.7 %reduce-scatter.5.cloned.1.call-start = ((), (), s32[]{:S(2)}) async-start(), calls=%async_computation.9 | async-start | bytes 294912 | tf_op jit(solution)/shard_map/reduce_scatter | solution.py:112
  140.8 58.9 %all-gather.5.cloned.1.call-start = ((), (), s32[]{:S(2)}) async-start(), calls=%async_computation.10 | async-start | bytes 2359296 | tf_op jit(solution)/shard_map/all_gather | solution.py:121
  141.4 103.8 %all-reduce.6.cloned.1.call-start = ((), (), s32[]{:S(2)}) async-start(), calls=%async_computation.11 | async-start | bytes 655360 | tf_op jit(solution)/shard_map/psum | solution.py:123
  160.4 41.9 %copy-start.8 = (f32[16,2]{0,1:T(2,128)S(1)}, f32[16,2]{0,1:T(2,128)}, u32[]{:S(2)}) copy-start(f32[16,2]{0,1:T(2,128)} %param.42) | copy-start | bytes 388
  160.4 41.9 %copy-start.9 = (f32[16]{0:T(128)S(1)}, f32[16]{0:T(128)}, u32[]{:S(2)}) copy-start(f32[16]{0:T(128)} %param.41) | copy-start | bytes 196
  160.4 89.5 %copy-start.6 = (bf16[2048]{0:T(1024)(128)(2,1)S(1)}, bf16[2048]{0:T(1024)(128)(2,1)}, u32[]{:S(2)}) copy-start(bf16[2048]{0:T(1024)(128)(2,1)} %param.39) | copy-start | bytes 12292
  245.2 15.7 %copy-start.4 = (bf16[16,2048]{1,0:T(8,128)(2,1)S(1)}, bf16[16,2048]{1,0:T(8,128)(2,1)}, u32[]{:S(2)}) copy-start(bf16[16,2048]{1,0:T(8,128)(2,1)} %get-tuple-element.5) | copy-start | bytes 196612
  245.2 14.4 %all-to-all-start.2 = ((bf16[8,8,2048]{2,1,0:T(8,128)(2,1)}), bf16[8,8,2048]{2,1,0:T(8,128)(2,1)S(1)}, u32[]{:S(2)}, u32[]{:S(2)}) async-start(bf16[8,8,2048]{2,1,0:T(8,128)(2,1)} %get-tuple-element.6), calls=%async_computation.3 | async-start | bytes 524288 | tf_op jit(solution)/shard_map/all_to_all | solution.py:148
Sparse Core Ops, SparseCore 0:
  23.2 30.4 reduce-scatter.2
  55.2 28.9 all-gather.2
  87.1 41.2 all-reduce.3
  140.9 28.6 reduce-scatter.4
  171.0 28.6 all-gather.4
  202.5 42.6 all-reduce.5
where the time goes:
time: 269 us; the launch traced here: 268 us
  waiting for transfers between devices  185 us (69%)
  blocking collectives  35.1 us (13%)
  matrix products  20.7 us (8%)
  between operations  13.8 us (5%)
  other arithmetic  6.95 us (3%)
  starting transfers between devices  4.98 us (2%)
    psum x1, waiting for transfers between devices, shards(): lax.psum(dense_terms.astype(jnp.bfloat16), 'tp').astype(jnp.float32)  42.8 us
    psum x1, waiting for transfers between devices, shards(): mixed_heads = lax.psum(head_terms, 'tp')  41.4 us
    all_gather x1, waiting for transfers between devices, shards(): lax.all_gather(dense_down_proj, 'ep', axis=1, tiled=True)  29.4 us
    reduce_scatter x1, waiting for transfers between devices, shards(): lax.psum_scatter(row_term(spread, joined), 'ep', scatter_dimension=0, til...  29.2 us
    all_gather x1, waiting for transfers between devices, shards(): lax.all_gather(output_weight, 'ep', axis=1, tiled=True)  22.4 us
    all_to_all x1, blocking collectives, shards(): lax.all_to_all(outbound, 'ep', split_axis=0, concat_axis=0, tiled=True)  12.7 us
    all_to_all x1, blocking collectives, shards(): lax.all_to_all(normed, 'ep', split_axis=1, concat_axis=0, tiled=True)  12.1 us
    all_to_all x1, blocking collectives, shards(): lax.all_to_all(ffn_in, 'ep', split_axis=1, concat_axis=0, tiled=True)  10.3 us
  transfers between devices with their start and end apart: 7, of which 7 were waited for; matrix products, arithmetic and copies ran while one was open for 6% of the time, Pallas kernels for 0%

commit v1 on v0

--- a/solution.py
+++ b/solution.py
@@ -103,7 +103,11 @@
     )
     attended = attended.reshape(seq_count, head_count * head_size)
     head_terms = right_product(attended, lax.all_gather(output_weight, "ep", axis=1, tiled=True))
-    mixed_heads = lax.psum(head_terms, "tp")
+    mixed_heads = head_terms
+    for hop in (1, 2):
+        mixed_heads = mixed_heads + lax.ppermute(
+            mixed_heads, "tp", [(dev, dev ^ hop) for dev in range(4)]
+        )
     residual = (tokens.astype(jnp.float32) + mixed_heads).astype(jnp.bfloat16)
     ffn_in = rms_scale(residual, ffn_gain).astype(jnp.bfloat16)
     dense_width = dense_gate_proj.shape[1]

time: 269 us -> 236 us (0.88)
  waiting for transfers between devices: 185 us -> 150 us
  starting transfers between devices: 4.98 us -> 7.81 us
    psum x1 -> x0, waiting for transfers between devices: 41.4 us -> none  [shards(): mixed_heads = lax.psum(head_terms, 'tp')]
    ppermute x0 -> x2, waiting for transfers between devices: none -> 7.8 us  [shards(): lax.ppermute(mixed_heads, 'tp', [(dev, dev ^ hop) for dev in range(4)])]
    ppermute x0 -> x2, starting transfers between devices: none -> 2.87 us  [shards(): lax.ppermute(mixed_heads, 'tp', [(dev, dev ^ hop) for dev in range(4)])]
  transfers between devices with their start and end apart: 7 -> 8, of which waited for: 7 -> 8; matrix products, arithmetic and copies ran while one was open for 6% -> 7% of each run, Pallas kernels for 0% -> 0%
where the time goes in v1:
time: 236 us; the launch traced here: 235 us
  waiting for transfers between devices  150 us (64%)
  blocking collectives  35.2 us (15%)
  matrix products  20 us (8%)
  between operations  13.4 us (6%)
  starting transfers between devices  7.81 us (3%)
  other arithmetic  6.07 us (3%)
    psum x1, waiting for transfers between devices, shards(): lax.psum(dense_terms.astype(jnp.bfloat16), 'tp').astype(jnp.float32)  42.8 us
    all_gather x1, waiting for transfers between devices, shards(): lax.all_gather(dense_down_proj, 'ep', axis=1, tiled=True)  29.5 us
    reduce_scatter x1, waiting for transfers between devices, shards(): lax.psum_scatter(row_term(spread, joined), 'ep', scatter_dimension=0, til...  29.2 us
    all_gather x1, waiting for transfers between devices, shards(): lax.all_gather(output_weight, 'ep', axis=1, tiled=True)  22.4 us
    all_to_all x1, blocking collectives, shards(): lax.all_to_all(outbound, 'ep', split_axis=0, concat_axis=0, tiled=True)  12.9 us
    all_to_all x1, blocking collectives, shards(): lax.all_to_all(normed, 'ep', split_axis=1, concat_axis=0, tiled=True)  12.1 us
    all_to_all x1, blocking collectives, shards(): lax.all_to_all(ffn_in, 'ep', split_axis=1, concat_axis=0, tiled=True)  10.2 us
    all_to_all x1, waiting for transfers between devices, shards(): lax.all_to_all(expert_result.reshape(sources, slots_now, feature).astype(...  9.53 us
  transfers between devices with their start and end apart: 8, of which 8 were waited for; matrix products, arithmetic and copies ran while one was open for 7% of the time, Pallas kernels for 0%

profile of v1, /device:TPU:0, one launch (start us, length us, event | category | flops | bytes accessed | tf_op | source)
XLA Modules:
  0.0 234.9 jit_solution(17800277466005070437)
XLA Ops:
  6.5 0.0 reduce-scatter.3.cloned.1.call-start
  6.6 1.1 fusion.32
  7.7 0.9 fusion.34
  8.7 12.1 %all_to_all.48 = bf16[16,8,256]{2,0,1:T(8,128)(2,1)S(1)} all-to-all(bf16[16,8,256]{2,0,1:T(8,128)(2,1)S(1)} %bitcast.96), channel_id=1, replica_groups=mesh['ep'=8,'tp'=4] {'ep'}, dimensions={1} | all-to-all | bytes 131072 | tf_op jit(solution)/shard_map/all_to_all | solution.py:87
  20.7 2.3 fusion.20
  23.0 0.0 reduce-scatter.3.cloned.1.call-update
  23.0 0.0 all-gather.3.cloned.1.call-start
  23.1 0.7 all-gather.3.cloned.1.call-update
  23.8 0.0 reduce-scatter.5.cloned.1.call-start
  23.8 0.0 copy-done.10
  23.8 0.1 iota_compare_fusion
  23.9 0.1 select_reduce_fusion
  24.0 0.1 copy.42
  24.1 0.1 fusion.70
  24.3 0.1 copy.43
  24.4 0.1 iota_compare_fusion.1
  24.4 29.2 %reduce-scatter.3.cloned.1.call-done = f32[16,1536]{1,0:T(8,128)} async-done(((f32[128,1536]{1,0:T(8,128)}), f32[16,1536]{1,0:T(8,128)}) %reduce-scatter.3.cloned.1.call-update) | async-done | bytes 98320 | tf_op jit(solution)/shard_map/reduce_scatter | solution.py:89
  53.6 0.9 convert.8
  54.6 0.1 multiply_reduce_fusion
  54.7 0.0 copy-start.1
  54.7 5.2 %fusion.80 = f32[16,4,1,384]{3,2,1,0:T(1,128)S(1)} fusion(bf16[16,4,128,1]{2,3,1,0:T(2,128)(2,1)S(1)} %reshape.151, bf16[16,4,384,128]{3,2,1,0:T(8,128)(2,1)} %param.30), kind=kOutput, calls=%fused_computation.117 | convolution fusion | flops 6291456 | bytes 6406144 | tf_op jit(solution)/shard_map/shd,shpd->shp/dot_general | solution.py:28
  59.9 0.2 fusion.78
  60.1 0.2 fusion.50
  60.3 0.1 fusion.52
  60.5 1.2 fusion.48
  61.7 0.0 copy-start.12
  61.7 0.1 add_convert_fusion
  61.8 22.4 %all-gather.3.cloned.1.call-done = bf16[512,2048]{1,0:T(8,128)(2,1)} async-done(((bf16[512,256]{1,0:T(8,128)(2,1)}), bf16[512,2048]{1,0:T(8,128)(2,1)}) %all-gather.3.cloned.1.call-update) | async-done | bytes 2097168 | tf_op jit(solution)/shard_map/all_gather | solution.py:105
  84.2 2.0 fusion.55
  86.2 1.4 collective-permute-start
  87.6 4.2 %collective-permute-done = f32[16,2048]{1,0:T(8,128)S(1)} collective-permute-done((f32[16,2048]{1,0:T(8,128)S(1)}, f32[16,2048]{1,0:T(8,128)S(1)}, u32[]{:S(2)}, u32[]{:S(2)}) %collective-permute-start) | collective-permute-done | bytes 131104 | tf_op jit(solution)/shard_map/ppermute | solution.py:108
  91.8 1.5 collective-permute-start.1
  93.3 3.6 %collective-permute-done.1 = f32[16,2048]{1,0:T(8,128)S(1)} collective-permute-done((f32[16,2048]{1,0:T(8,128)S(1)}, f32[16,2048]{1,0:T(8,128)S(1)}, u32[]{:S(2)}, u32[]{:S(2)}) %collective-permute-start.1) | collective-permute-done | bytes 131104 | tf_op jit(solution)/shard_map/ppermute | solution.py:108
  96.9 0.1 fusion.36
  97.0 0.1 fusion.38
  97.1 10.2 %all_to_all.49 = bf16[16,8,256]{2,0,1:T(8,128)(2,1)S(1)} all-to-all(bf16[16,8,256]{2,0,1:T(8,128)(2,1)S(1)} %bitcast.97), channel_id=1, replica_groups=mesh['ep'=8,'tp'=4] {'ep'}, dimensions={1} | all-to-all | bytes 131072 | tf_op jit(solution)/shard_map/all_to_all | solution.py:114
  107.4 0.9 convolution_convert_fusion.3
  108.3 0.0 reduce-scatter.5.cloned.1.call-update
  108.3 0.0 all-gather.5.cloned.1.call-start
  108.4 0.5 all-gather.5.cloned.1.call-update
  108.9 0.0 all-reduce.3.cloned.1.call-start
  109.0 0.1 copy.44
  109.0 0.1 eq.62
  109.1 0.1 fusion.59
  109.2 0.1 reduce_window_sum.11
  109.3 0.2 select_reduce_fusion.1
  109.5 0.1 reduce_sum.71
  109.5 0.1 copy.45
  109.6 0.3 fusion
  110.0 12.9 %all_to_all.50 = bf16[8,8,2048]{2,1,0:T(8,128)(2,1)S(1)} all-to-all(bf16[8,8,2048]{2,1,0:T(8,128)(2,1)S(1)} %fusion), channel_id=1, replica_groups=mesh['ep'=8,'tp'=4] {'ep'}, dimensions={0} | all-to-all | bytes 524288 | tf_op jit(solution)/shard_map/all_to_all | solution.py:144
  122.9 2.1 fusion.5
  125.0 3.2 %fusion.1 = bf16[8,8,2048]{2,1,0:T(8,128)(2,1)} fusion(bf16[1,512,2048]{2,1,0:T(8,128)(2,1)S(1)} %copy-done, bf16[1,2048,512]{2,1,0:T(8,128)(2,1)} %param.44, bf16[8,8,2048]{2,1,0:T(8,128)(2,1)S(1)} %all_to_all.50, f32[64,512]{1,0:T(8,128)S(1)} %fusion.5), kind=kOutput, calls=%fused_computation.5 | convolution fusion | flops 268763136 | bytes 4849664 | tf_op jit(solution)/shard_map/dot_general | solution.py:150
  128.2 8.0 %reduce-scatter.5.cloned.1.call-done = bf16[16,1024]{1,0:T(8,128)(2,1)} async-done(((bf16[128,1024]{1,0:T(8,128)(2,1)}), bf16[16,1024]{1,0:T(8,128)(2,1)}) %reduce-scatter.5.cloned.1.call-update) | async-done | bytes 32784 | tf_op jit(solution)/shard_map/reduce_scatter | solution.py:116
  136.1 0.8 convert_element_type.119
  136.9 29.5 %all-gather.5.cloned.1.call-done = bf16[512,2048]{1,0:T(8,128)(2,1)} async-done(((bf16[512,256]{1,0:T(8,128)(2,1)}), bf16[512,2048]{1,0:T(8,128)(2,1)}) %all-gather.5.cloned.1.call-update) | async-done | bytes 2097168 | tf_op jit(solution)/shard_map/all_gather | solution.py:125
  166.4 2.6 %convolution_convert_fusion.2 = bf16[16,2048]{1,0:T(8,128)(2,1)} fusion(bf16[512,2048]{1,0:T(8,128)(2,1)} %all-gather.5.cloned.1.call-done, f32[16,1024]{1,0:T(8,128)S(1)} %convert_element_type.119), kind=kOutput, calls=%fused_computation.6 | convolution fusion | flops 33636352 | bytes 2228224 | tf_op jit(solution)/shard_map/dot_general | solution.py:54
  169.0 0.0 all-reduce.3.cloned.1.call-update
  169.1 42.8 %all-reduce.3.cloned.1.call-done = (bf16[16,2048]{1,0:T(8,128)(2,1)}, bf16[8,8,2048]{2,1,0:T(8,128)(2,1)}) async-done(((bf16[16,2048]{1,0:T(8,128)(2,1)}, bf16[8,8,2048]{2,1,0:T(8,128)(2,1)}), (bf16[16,2048]{1,0:T(8,128)(2,1)}, bf16[8,8,2048]{2,1,0:T(8,128)(2,1)})) %all-reduce.3.cloned.1.call-update) | async-done | bytes 327696 | tf_op jit(solution)/shard_map/psum | solution.py:127
  211.9 4.7 %all-to-all-start.2 = ((bf16[8,8,2048]{2,1,0:T(8,128)(2,1)}), bf16[8,8,2048]{2,1,0:T(8,128)(2,1)S(1)}, u32[]{:S(2)}, u32[]{:S(2)}) async-start(bf16[8,8,2048]{2,1,0:T(8,128)(2,1)} %get-tuple-element.6), calls=%async_computation.3 | async-start | bytes 524288 | tf_op jit(solution)/shard_map/all_to_all | solution.py:152
  216.7 0.1 fusion.17
  216.8 9.5 %all-to-all-done.2 = bf16[8,8,2048]{2,1,0:T(8,128)(2,1)S(1)} async-done(((bf16[8,8,2048]{2,1,0:T(8,128)(2,1)}), bf16[8,8,2048]{2,1,0:T(8,128)(2,1)S(1)}, u32[]{:S(2)}, u32[]{:S(2)}) %all-to-all-start.2) | async-done | bytes 262176 | tf_op jit(solution)/shard_map/all_to_all | solution.py:152
  226.4 0.6 gather_fusion
  227.0 0.6 gather_fusion.1
  227.6 0.7 fusion.39
  (48 shorter events, 0.3 us)
Async XLA Ops:
  6.5 118.4 %copy-start = (bf16[1,512,2048]{2,1,0:T(8,128)(2,1)S(1)}, bf16[1,512,2048]{2,1,0:T(8,128)(2,1)}, u32[]{:S(2)}) copy-start(bf16[1,512,2048]{2,1,0:T(8,128)(2,1)} %param.45) | copy-start | bytes 6291460
  6.5 17.3 %copy-start.10 = (s32[16]{0:T(128)S(1)}, s32[16]{0:T(128)}, u32[]{:S(2)}) copy-start(s32[16]{0:T(128)} %param.33) | copy-start | bytes 196
  6.5 17.4 %copy-start.3 = (f32[16,4,384]{2,1,0:T(4,128)S(1)}, f32[16,4,384]{2,1,0:T(4,128)}, u32[]{:S(2)}) copy-start(f32[16,4,384]{2,1,0:T(4,128)} %param.32) | copy-start | bytes 294916
  6.5 17.6 %copy-start.13 = (bf16[2048,4]{0,1:T(4,128)(2,1)S(1)}, bf16[2048,4]{0,1:T(4,128)(2,1)}, u32[]{:S(2)}) copy-start(bf16[2048,4]{0,1:T(4,128)(2,1)} %param.28) | copy-start | bytes 49156
  6.5 17.6 %copy-start.14 = (f32[4]{0:T(128)S(1)}, f32[4]{0:T(128)}, u32[]{:S(2)}) copy-start(f32[4]{0:T(128)} %param.29) | copy-start | bytes 52
  6.5 47.1 %reduce-scatter.3.cloned.1.call-start = ((), (), s32[]{:S(2)}) async-start(), calls=%async_computation.6 | async-start | bytes 884736 | tf_op jit(solution)/shard_map/reduce_scatter | solution.py:89
  23.0 61.2 %all-gather.3.cloned.1.call-start = ((), (), s32[]{:S(2)}) async-start(), calls=%async_computation.7 | async-start | bytes 2359296 | tf_op jit(solution)/shard_map/all_gather | solution.py:105
  23.8 112.4 %reduce-scatter.5.cloned.1.call-start = ((), (), s32[]{:S(2)}) async-start(), calls=%async_computation.8 | async-start | bytes 294912 | tf_op jit(solution)/shard_map/reduce_scatter | solution.py:116
  54.7 5.8 %copy-start.1 = (bf16[16,4,384,128]{3,2,1,0:T(8,128)(2,1)S(1)}, bf16[16,4,384,128]{3,2,1,0:T(8,128)(2,1)}, u32[]{:S(2)}) copy-start(bf16[16,4,384,128]{3,2,1,0:T(8,128)(2,1)} %param.31) | copy-start | bytes 18874372
  61.6 35.2 %copy-start.2 = (bf16[16,2048]{1,0:T(8,128)(2,1)S(1)}, bf16[16,2048]{1,0:T(8,128)(2,1)}, u32[]{:S(2)}) copy-start(bf16[16,2048]{1,0:T(8,128)(2,1)} %param.23) | copy-start | bytes 196612
  61.6 35.4 %copy-start.5 = (f32[2048]{0:T(1024)S(1)}, f32[2048]{0:T(1024)}, u32[]{:S(2)}) copy-start(f32[2048]{0:T(1024)} %param.35) | copy-start | bytes 24580
  61.6 45.7 %copy-start.11 = (bf16[256,512]{1,0:T(8,128)(2,1)S(1)}, bf16[256,512]{1,0:T(8,128)(2,1)}, u32[]{:S(2)}) copy-start(bf16[256,512]{1,0:T(8,128)(2,1)} %param.37) | copy-start | bytes 786436
  61.7 45.7 %copy-start.12 = (bf16[256,512]{1,0:T(8,128)(2,1)S(1)}, bf16[256,512]{1,0:T(8,128)(2,1)}, u32[]{:S(2)}) copy-start(bf16[256,512]{1,0:T(8,128)(2,1)} %param.36) | copy-start | bytes 786436
  84.2 24.8 %copy-start.7 = (s32[16,2]{0,1:T(2,128)S(1)}, s32[16,2]{0,1:T(2,128)}, u32[]{:S(2)}) copy-start(s32[16,2]{0,1:T(2,128)} %param.40) | copy-start | bytes 388
  86.2 5.6 %collective-permute-start = (f32[16,2048]{1,0:T(8,128)S(1)}, f32[16,2048]{1,0:T(8,128)S(1)}, u32[]{:S(2)}, u32[]{:S(2)}) collective-permute-start(f32[16,2048]{1,0:T(8,128)S(1)} %fusion.55), channel_id=1, source_target_pairs={{0,1},{1,0},{2,3},{3,2},{4,5},{5,4},{6,7},{7,6},{8,9},{9,8},{10,11... | collective-permute-start | bytes 393224 | tf_op jit(solution)/shard_map/ppermute | solution.py:108
  91.8 5.0 %collective-permute-start.1 = (f32[16,2048]{1,0:T(8,128)S(1)}, f32[16,2048]{1,0:T(8,128)S(1)}, u32[]{:S(2)}, u32[]{:S(2)}) collective-permute-start(f32[16,2048]{1,0:T(8,128)S(1)} %add.116), channel_id=1, source_target_pairs={{0,2},{1,3},{2,0},{3,1},{4,6},{5,7},{6,4},{7,5},{8,10},{9,11},{10,... | collective-permute-start | bytes 393224 | tf_op jit(solution)/shard_map/ppermute | solution.py:108
  108.3 58.1 %all-gather.5.cloned.1.call-start = ((), (), s32[]{:S(2)}) async-start(), calls=%async_computation.9 | async-start | bytes 2359296 | tf_op jit(solution)/shard_map/all_gather | solution.py:125
  108.9 103.0 %all-reduce.3.cloned.1.call-start = ((), (), s32[]{:S(2)}) async-start(), calls=%async_computation.10 | async-start | bytes 655360 | tf_op jit(solution)/shard_map/psum | solution.py:127
  128.2 40.9 %copy-start.8 = (f32[16,2]{0,1:T(2,128)S(1)}, f32[16,2]{0,1:T(2,128)}, u32[]{:S(2)}) copy-start(f32[16,2]{0,1:T(2,128)} %param.42) | copy-start | bytes 388
  128.2 40.9 %copy-start.9 = (f32[16]{0:T(128)S(1)}, f32[16]{0:T(128)}, u32[]{:S(2)}) copy-start(f32[16]{0:T(128)} %param.41) | copy-start | bytes 196
  128.2 88.5 %copy-start.6 = (bf16[2048]{0:T(1024)(128)(2,1)S(1)}, bf16[2048]{0:T(1024)(128)(2,1)}, u32[]{:S(2)}) copy-start(bf16[2048]{0:T(1024)(128)(2,1)} %param.39) | copy-start | bytes 12292
  211.9 15.7 %copy-start.4 = (bf16[16,2048]{1,0:T(8,128)(2,1)S(1)}, bf16[16,2048]{1,0:T(8,128)(2,1)}, u32[]{:S(2)}) copy-start(bf16[16,2048]{1,0:T(8,128)(2,1)} %get-tuple-element.5) | copy-start | bytes 196612
  211.9 14.4 %all-to-all-start.2 = ((bf16[8,8,2048]{2,1,0:T(8,128)(2,1)}), bf16[8,8,2048]{2,1,0:T(8,128)(2,1)S(1)}, u32[]{:S(2)}, u32[]{:S(2)}) async-start(bf16[8,8,2048]{2,1,0:T(8,128)(2,1)} %get-tuple-element.6), calls=%async_computation.3 | async-start | bytes 524288 | tf_op jit(solution)/shard_map/all_to_all | solution.py:152
Sparse Core Ops, SparseCore 0:
  23.1 30.4 reduce-scatter.2
  55.2 28.9 all-gather.2
  108.4 27.6 reduce-scatter.4
  137.6 28.7 all-gather.4
  169.2 42.6 all-reduce.2
